TPU v7x, 32 devices: a whole 2x2x4 slice. The times are simulated.
32 devices in a mesh: sp: 8 (over z, y), tp: 4 (over x, core).
Axes of the slice: x: 2, y: 2, z: 4, core: 2. Of those that a mesh axis runs over, the one named last changes fastest.
Arguments:
- residual_in: bfloat16 [8192, 2048], P(('sp', 'tp')), may hold values from -6 to 6
- queries: bfloat16 [8192, 2048], P('sp', 'tp'), may hold values from -6 to 6
- keys: bfloat16 [8192, 1024], P('sp', 'tp'), may hold values from -6 to 6
- values: bfloat16 [8192, 1024], P('sp', 'tp'), may hold values from -6 to 6
- query_gain: float32 [128], replicated, may hold values from 1 to 7
- key_norm_gain: float32 [128], replicated, may hold values from 1 to 7
- out_weight: bfloat16 [2048, 2048], replicated, may hold values from -0.125 to 0.125
- norm_gain: float32 [2048], replicated, may hold values from 0.1 to 1.9
- up_weight: bfloat16 [2048, 8192], P('sp', 'tp'), may hold values from -0.125 to 0.125
- down_weight: bfloat16 [8192, 2048], P('tp', 'sp'), may hold values from -0.0625 to 0.0625
Outputs:
- residual_out: bfloat16 [8192, 2048], P(('sp', 'tp'))
All inputs are finite; a program needn't handle non-finite values.
Results may differ from a plain program's by a relative error of at most 0.017.
The roundings to bfloat16 on the way count: a program that leaves them out, or rounds other values in their place, can miss the bound.
Values may be sent and summed in bfloat16 or wider, within the bound.
A program may use at most 128 MiB of HBM per device.

v0:
```python
import functools

import jax
import jax.numpy as jnp
import numpy as np
from jax import lax
from jax.experimental import pallas as pl
from jax.experimental.pallas import tpu as pltpu
from jax.sharding import PartitionSpec as P

HEAD_WIDTH = 128
GRID_W = 64
epsilon = 1e-06
MESH = pl.DeviceIdType.MESH
VALUE, KEY, UP, DOWN = range(4)


def ring_order(mesh):
    count = mesh.shape["sp"]
    width = 0
    try:
        width = len({device.coords[1] for device in mesh.devices.flat})
    except Exception:
        width = 0
    if width < 2 or count % width or (count // width) % 2:
        width = 2
        while width * width < count // 2:
            width *= 2
    depth = count // width
    order = [z * width for z in range(depth)]
    for z in reversed(range(depth)):
        columns = list(range(1, width))
        if (depth - 1 - z) % 2:
            columns.reverse()
        order += [z * width + y for y in columns]
    return order


def lookup(table, index):
    found = jnp.int32(table[0])
    for i, entry in enumerate(table):
        if i:
            found = jnp.where(index == i, jnp.int32(entry), found)
    return found


def rotary_tables(tokens):
    quarter = HEAD_WIDTH // 4
    exponent = -np.arange(quarter, dtype=np.float32) / np.float32(quarter)
    inverse = np.power(np.float64(10000.0), exponent.astype(np.float64)).astype(np.float32)
    sign = np.concatenate([-np.ones(quarter), np.ones(quarter)])

    def parts(count):
        angle = np.arange(count, dtype=np.float32)[:, None] * inverse
        twice = np.concatenate([angle, angle], axis=-1).astype(np.float64)
        return np.cos(twice), np.sin(twice) * sign

    row_cos, row_sin = parts(tokens // GRID_W)
    col_cos, col_sin = parts(GRID_W)
    left = lambda a: jnp.asarray(np.pad(a, ((0, 0), (0, HEAD_WIDTH // 2))).astype(np.float32))
    right = lambda a: jnp.asarray(np.pad(a, ((0, 0), (HEAD_WIDTH // 2, 0))).astype(np.float32))
    return left(row_cos), left(row_sin), right(col_cos), right(col_sin)


def layer_kernel(
    order, tp, residual, queries, keys, values, query_gain, key_gain, row_cos, row_sin, col_cos, col_sin,
    out_weight, norm_gain, up, down, out,
    key_raw, key_own, value_own, up_own, down_own, key_buf, value_buf, up_buf, down_buf, query, attn,
    acc, best, mass, heads, weight, middle, normed, give, take, rest,
    load_sem, ring_send, ring_recv, head_send, head_recv, norm_send, norm_recv, part_send, part_recv,
):
    count = len(order)
    half = count // 2
    me = lax.axis_index("sp")
    rank = lax.axis_index("tp")
    position = {sp: i for i, sp in enumerate(order)}
    at_distance = lambda d: lookup([order[(position[i] + d) % count] for i in range(count)], me)
    target = (at_distance(1), at_distance(-1))
    peer = [rank] + [lookup([i ^ k for i in range(tp)], rank) for k in range(1, tp)]
    far_first = sorted(range(1, tp), key=lambda k: (k < 2, k))

    rows = query.shape[0]
    own_rows = heads.shape[0]
    kv_heads = key_own.shape[1] // HEAD_WIDTH
    q_heads = query.shape[1] // HEAD_WIDTH
    group = q_heads // kv_heads
    tile = min(256, rows)
    scale = HEAD_WIDTH ** (-0.5) * 1.4426950408889634

    loads = [
        pltpu.make_async_copy(src, dst, load_sem.at[i])
        for i, (src, dst) in enumerate((
            (values, value_own), (keys, key_raw), (up, up_own), (queries, attn),
            (down, down_own), (residual, rest), (out_weight, weight),
        ))
    ]
    for load in loads:
        load.start()

    barrier = pltpu.get_barrier_semaphore()
    for device in target:
        pl.semaphore_signal(barrier, inc=1, device_id={"sp": device}, device_id_type=MESH)
    for k in range(1, tp):
        pl.semaphore_signal(barrier, inc=1, device_id={"tp": peer[k]}, device_id_type=MESH)
    pl.semaphore_wait(barrier, 1 + tp)

    rings = ((value_own, value_buf), (key_own, key_buf), (up_own, up_buf), (down_own, down_buf))

    def slot(way, step):
        return (half - 1) * way + step - 1 if step < half else count - 2

    def exists(way, step, part):
        return step < half or (step == half and part == way)

    def ring(kind, way, step, part):
        own, buf = rings[kind]
        size = own.shape[0] // 2
        span = pl.ds(part * size, size)
        return pltpu.make_async_remote_copy(
            src_ref=own.at[span] if step == 1 else buf.at[slot(way, step - 1), span],
            dst_ref=buf.at[slot(way, step), span],
            send_sem=ring_send.at[kind, way, step - 1, part],
            recv_sem=ring_recv.at[kind, way, step - 1, part],
            device_id={"sp": target[way]},
            device_id_type=MESH,
        )

    def launch(kind):
        for part in (0, 1):
            for way in (0, 1):
                ring(kind, way, 1, part).start()

    def relay(kind, step):
        for part in (0, 1):
            for way in (0, 1):
                if exists(way, step, part):
                    ring(kind, way, step, part).wait_recv()
                    if exists(way, step + 1, part):
                        ring(kind, way, step + 1, part).start()

    def rotate(src, gain, dst):
        lane = lax.broadcasted_iota(jnp.int32, (GRID_W, HEAD_WIDTH), 1)
        even = (lane // (HEAD_WIDTH // 4)) % 2 == 0

        def body(r, carry):
            grid_row = me * (rows // GRID_W) + r
            cosine = col_cos[...] + row_cos[pl.ds(grid_row, 1), :]
            sine = col_sin[...] + row_sin[pl.ds(grid_row, 1), :]
            here = pl.ds(pl.multiple_of(r * GRID_W, GRID_W), GRID_W)
            for h in range(src.shape[1] // HEAD_WIDTH):
                cols = pl.ds(h * HEAD_WIDTH, HEAD_WIDTH)
                v = src[here, cols].astype(jnp.float32)
                v = v * lax.rsqrt(jnp.mean(v * v, axis=-1, keepdims=True) + epsilon) * gain[...]
                turned = jnp.where(
                    even,
                    pltpu.roll(v, HEAD_WIDTH - HEAD_WIDTH // 4, 1),
                    pltpu.roll(v, HEAD_WIDTH // 4, 1),
                )
                dst[here, cols] = (v * cosine + turned * sine).astype(dst.dtype)
            return carry

        lax.fori_loop(0, rows // GRID_W, body, 0)

    def flash(key_at, value_at, first):
        def body(index, carry):
            per_head = rows // tile
            kv = index // per_head
            here = pl.ds(pl.multiple_of((index % per_head) * tile, tile), tile)
            kv_cols = pl.ds(pl.multiple_of(kv * HEAD_WIDTH, HEAD_WIDTH), HEAD_WIDTH)
            key = key_at[:, kv_cols]
            value = value_at[:, kv_cols]

            def column(g):
                return pl.ds(pl.multiple_of((kv * group + g) * HEAD_WIDTH, HEAD_WIDTH), HEAD_WIDTH)

            def score(g):
                return lax.dot_general(
                    query[here, column(g)], key, (((1,), (1,)), ((), ())),
                    preferred_element_type=jnp.float32,
                )

            scores = [score(g) for g in range(group)]
            for g in range(group):
                s = scores[g]
                cols = column(g)
                top = jnp.max(s, axis=1, keepdims=True) * scale
                if first:
                    newest = jnp.broadcast_to(top, (tile, HEAD_WIDTH))
                else:
                    old = best[here, cols]
                    newest = jnp.maximum(old, top)
                    factor = jnp.exp2(old - newest)
                p = jnp.exp2(s * scale - newest[:, :1])
                total = jnp.sum(p, axis=1, keepdims=True)
                part = jnp.dot(p.astype(jnp.bfloat16), value, preferred_element_type=jnp.float32)
                best[here, cols] = newest
                if first:
                    mass[here, cols] = jnp.broadcast_to(total, (tile, HEAD_WIDTH))
                    acc[here, cols] = part
                else:
                    mass[here, cols] = mass[here, cols] * factor + total
                    acc[here, cols] = acc[here, cols] * factor + part
            return carry

        lax.fori_loop(0, kv_heads * (rows // tile), body, 0)

    loads[0].wait()
    launch(VALUE)
    loads[1].wait()
    rotate(key_raw, key_gain, key_own)
    launch(KEY)
    loads[2].wait()
    launch(UP)
    loads[3].wait()
    rotate(attn, query_gain, query)
    flash(key_own, value_own, True)
    for step in range(1, half + 1):
        relay(VALUE, step)
        relay(KEY, step)
        if step == half - 1:
            relay(UP, 1)
        for way in (0, 1) if step < half else (0,):
            flash(key_buf.at[slot(way, step)], value_buf.at[slot(way, step)], False)

    width = query.shape[1]
    mine = pl.ds(pl.multiple_of(rank * width, width), width)

    def token_rows(k):
        return pl.ds(pl.multiple_of(peer[k] * own_rows, own_rows), own_rows)

    def head_copy(k):
        return pltpu.make_async_remote_copy(
            src_ref=attn.at[token_rows(k)],
            dst_ref=heads.at[:, mine],
            send_sem=head_send.at[k - 1],
            recv_sem=head_recv.at[k - 1],
            device_id={"tp": peer[k]},
            device_id_type=MESH,
        )

    for k in far_first:
        attn[token_rows(k), :] = (acc[token_rows(k), :] / mass[token_rows(k), :]).astype(attn.dtype)
        head_copy(k).start()
    heads[:, mine] = (acc[token_rows(0), :] / mass[token_rows(0), :]).astype(heads.dtype)

    def head_arrival(k):
        cols = pl.ds(pl.multiple_of(peer[k] * width, width), width)
        return pltpu.make_async_remote_copy(
            src_ref=attn.at[token_rows(k)],
            dst_ref=heads.at[:, cols],
            send_sem=head_send.at[k - 1],
            recv_sem=head_recv.at[k - 1],
            device_id={"tp": peer[k]},
            device_id_type=MESH,
        )

    if half > 2:
        relay(UP, 2)
    for load in loads[4:]:
        load.wait()
    for k in range(1, tp):
        head_arrival(k).wait_recv()

    features = middle.shape[1]
    lanes = min(256, features)

    def feature_cols(c):
        return pl.ds(pl.multiple_of(c * lanes, lanes), lanes)

    def project(c, total):
        cols = feature_cols(c)
        made = rest[:, cols].astype(jnp.float32) + jnp.dot(
            heads[...], weight[:, cols], preferred_element_type=jnp.float32
        )
        middle[:, cols] = made
        return total + jnp.sum(made * made, axis=1, keepdims=True)

    squares = lax.fori_loop(0, features // lanes, project, jnp.zeros((own_rows, 1), jnp.float32))
    inverse = lax.rsqrt(squares / features + epsilon)

    def normalize(c, carry):
        cols = feature_cols(c)
        normed[pl.ds(0, own_rows), cols] = (middle[:, cols] * inverse * norm_gain[:, cols]).astype(normed.dtype)
        return carry

    lax.fori_loop(0, features // lanes, normalize, 0)

    def rows_of(k):
        return pl.ds(k * own_rows, own_rows)

    def norm_copy(k):
        source = 0 if k % 2 == 0 else k - 1
        return pltpu.make_async_remote_copy(
            src_ref=normed.at[rows_of(source)],
            dst_ref=normed.at[rows_of(k)],
            send_sem=norm_send.at[k - 1],
            recv_sem=norm_recv.at[k - 1],
            device_id={"tp": peer[k if k % 2 == 0 else 1]},
            device_id_type=MESH,
        )

    for k in range(2, tp, 2):
        norm_copy(k).start()
    norm_copy(1).start()
    for step in range(3, half):
        relay(UP, step)
    launch(DOWN)
    for k in range(2, tp, 2):
        norm_copy(k).wait_recv()
        norm_copy(k + 1).start()
    for k in range(1, tp, 2):
        norm_copy(k).wait_recv()
    relay(UP, half)

    blocks = [(me, None)]
    for step in range(1, half + 1):
        for way in (0, 1) if step < half else (0,):
            blocks.append((at_distance(step if way else -step), slot(way, step)))

    depth = up_own.shape[0]
    hidden = up_own.shape[1]
    all_rows = tp * own_rows
    row_tile = all_rows // 2
    hid_tile = min(256, hidden)
    act = weight.at[pl.ds(0, all_rows), pl.ds(0, hidden)]

    def units(i, carry):
        here = pl.ds(pl.multiple_of((i % 2) * row_tile, row_tile), row_tile)
        cols = pl.ds(pl.multiple_of((i // 2) * hid_tile, hid_tile), hid_tile)
        total = None
        for source, place in blocks:
            there = pl.ds(pl.multiple_of(source * depth, depth), depth)
            matrix = up_own[:, cols] if place is None else up_buf[place, :, cols]
            product = jnp.dot(normed[here, there], matrix, preferred_element_type=jnp.float32)
            total = product if total is None else total + product
        total = jnp.maximum(total, 0.0)
        act[here, cols] = (total * total).astype(act.dtype)
        return carry

    lax.fori_loop(0, 2 * (hidden // hid_tile), units, 0)

    out_cols = down_own.shape[1]

    def part_copy(c, k):
        return pltpu.make_async_remote_copy(
            src_ref=give.at[c, rows_of(k)],
            dst_ref=take.at[c, rows_of(k - 1)],
            send_sem=part_send.at[c, k - 1],
            recv_sem=part_recv.at[c, k - 1],
            device_id={"tp": peer[k]},
            device_id_type=MESH,
        )

    def contribute(c):
        source, place = blocks[c]
        matrix = down_own[...] if place is None else down_buf[place]
        for low in (row_tile, 0):
            here = pl.ds(low, row_tile)
            give[c, here, :] = jnp.dot(act[here, :], matrix, preferred_element_type=jnp.float32).astype(give.dtype)
            for k in range(1, tp):
                if low <= k * own_rows < low + row_tile:
                    part_copy(c, k).start()
        cols = pl.ds(pl.multiple_of(source * out_cols, out_cols), out_cols)
        middle[:, cols] += give[c, rows_of(0), :].astype(jnp.float32)

    def finish(c):
        source, place = blocks[c]
        cols = pl.ds(pl.multiple_of(source * out_cols, out_cols), out_cols)
        total = middle[:, cols]
        for k in range(1, tp):
            part_copy(c, k).wait_recv()
            total = total + take[c, rows_of(k - 1), :].astype(jnp.float32)
        out[:, cols] = total.astype(out.dtype)

    contribute(0)
    done = 0
    ready = 1
    for step in range(1, half + 1):
        relay(DOWN, step)
        fresh = 2 if step < half else 1
        for c in range(ready, ready + fresh):
            contribute(c)
        for c in range(done, ready):
            finish(c)
        done, ready = ready, ready + fresh
    for c in range(done, ready):
        finish(c)

    for kind in range(4):
        for step in range(1, half + 1):
            for part in (0, 1):
                for way in (0, 1):
                    if exists(way, step, part):
                        ring(kind, way, step, part).wait_send()
    for k in range(1, tp):
        head_copy(k).wait_send()
        norm_copy(k).wait_send()
        for c in range(count):
            part_copy(c, k).wait_send()


def local(
    order, tp, residual_in, queries, keys, values, query_gain, key_norm_gain, out_weight, norm_gain, up_weight, down_weight
):
    count = len(order)
    rows, width = queries.shape
    own_rows, features = residual_in.shape
    tables = rotary_tables(rows * count)
    anywhere = pl.BlockSpec(memory_space=pl.ANY)
    vmem = pl.BlockSpec(memory_space=pltpu.VMEM)
    bf16, f32 = jnp.bfloat16, jnp.float32
    others = lambda a: pltpu.VMEM((count - 1,) + a.shape, bf16)
    dma = pltpu.SemaphoreType.DMA
    return pl.pallas_call(
        functools.partial(layer_kernel, order, tp),
        out_shape=jax.ShapeDtypeStruct(residual_in.shape, bf16),
        in_specs=[anywhere] * 4 + [vmem] * 6 + [anywhere, vmem, anywhere, anywhere],
        out_specs=vmem,
        scratch_shapes=[
            pltpu.VMEM(keys.shape, bf16),
            pltpu.VMEM(keys.shape, bf16),
            pltpu.VMEM(values.shape, bf16),
            pltpu.VMEM(up_weight.shape, bf16),
            pltpu.VMEM(down_weight.shape, bf16),
            others(keys),
            others(values),
            others(up_weight),
            others(down_weight),
            pltpu.VMEM(queries.shape, bf16),
            pltpu.VMEM(queries.shape, bf16),
            pltpu.VMEM(queries.shape, f32),
            pltpu.VMEM(queries.shape, f32),
            pltpu.VMEM(queries.shape, f32),
            pltpu.VMEM((own_rows, width * tp), bf16),
            pltpu.VMEM(out_weight.shape, bf16),
            pltpu.VMEM(residual_in.shape, f32),
            pltpu.VMEM((tp * own_rows, features), bf16),
            pltpu.VMEM((count, tp * own_rows, down_weight.shape[1]), bf16),
            pltpu.VMEM((count, (tp - 1) * own_rows, down_weight.shape[1]), bf16),
            pltpu.VMEM(residual_in.shape, bf16),
            dma((7,)),
            dma((4, 2, count // 2, 2)),
            dma((4, 2, count // 2, 2)),
            dma((tp - 1,)),
            dma((tp - 1,)),
            dma((tp - 1,)),
            dma((tp - 1,)),
            dma((count, tp - 1)),
            dma((count, tp - 1)),
        ],
        compiler_params=pltpu.CompilerParams(
            collective_id=0, has_side_effects=True, vmem_limit_bytes=67043328
        ),
        name="layer",
    )(
        residual_in, queries, keys, values, query_gain[None], key_norm_gain[None], *tables,
        out_weight, norm_gain[None], up_weight, down_weight,
    )


def solution(mesh):
    return jax.shard_map(
        functools.partial(local, ring_order(mesh), mesh.shape["tp"]),
        mesh=mesh,
        in_specs=(
            P(("sp", "tp"), None),
            P("sp", "tp"),
            P("sp", "tp"),
            P("sp", "tp"),
            P(),
            P(),
            P(),
            P(),
            P("sp", "tp"),
            P("tp", "sp"),
        ),
        out_specs=P(("sp", "tp"), None),
        check_vma=False,
    )
```

profile of v0, /device:TPU:0, one launch (start us, length us, event | category | flops | bytes accessed | tf_op | source)
XLA Modules:
  0.0 256.3 jit_solution(17429626175622478312)
XLA Ops:
  0.0 254.0 %layer.1 = bf16[256,2048]{1,0:T(8,128)(2,1)} custom-call(bf16[256,2048]{1,0:T(8,128)(2,1)} %residual.1, bf16[1024,512]{1,0:T(8,128)(2,1)} %queries.1, bf16[1024,256]{1,0:T(8,128)(2,1)} %keys.1, bf16[1024,256]{1,0:T(8,128)(2,1)} %values.1, f32[1,128]{1,0:T(1,128)} %bitcast.4, f32[1,128]{1,0:T(1,128)} %bitcast.5, f32[128,128]{1,0:T(8,128)} %constant.8.clone.row_cos, ...), custom_call_target="tpu_custom_call" | custom-call | tf_op jit(solution)/shard_map/layer/pallas_call | solution.py:414
  254.0 2.3 copy.16
where the time goes:
time: 257 us; the launch traced here: 256 us
  Pallas kernels  254 us (99%)
    pallas_call x1, Pallas kernels, local(): pl.pallas_call(functools.partial(layer_kernel, order, tp), out_shape=jax....  254 us

commit v1 on v0

--- a/solution.py
+++ b/solution.py
@@ -15,7 +15,7 @@
 VALUE, KEY, UP, DOWN = range(4)
 
 
-def ring_order(mesh):
+def plane_width(mesh):
     count = mesh.shape["sp"]
     width = 0
     try:
@@ -26,6 +26,12 @@
         width = 2
         while width * width < count // 2:
             width *= 2
+    return width
+
+
+def ring_order(mesh):
+    count = mesh.shape["sp"]
+    width = plane_width(mesh)
     depth = count // width
     order = [z * width for z in range(depth)]
     for z in reversed(range(depth)):
@@ -458,9 +464,546 @@
     )
 
 
+def paired_kernel(
+    depth, tp, residual, queries, keys, values, query_gain, key_gain, row_cos, row_sin, col_cos, col_sin,
+    out_weight, norm_gain, up, down, out,
+    key_raw, key_spare, key_all, value_all, query_raw, query_spare, query, attn, acc, best, mass, heads,
+    weight, middle, normed, up_all, down_all, give, sibling, take, rest,
+    load_sem, line_send, line_recv, swap_send, swap_recv, head_send, head_recv, norm_send, norm_recv,
+    core_send, core_recv, part_send, part_recv,
+):
+    me = lax.axis_index("sp")
+    rank = lax.axis_index("tp")
+    layer = me // 2
+    row = me % 2
+    mate = me + 1 - 2 * row
+    place = (me, mate)
+    side = (row, 1 - row)
+    peer = [rank] + [lookup([i ^ k for i in range(tp)], rank) for k in range(1, tp)]
+    pairs = [(j, k) for k in range(tp) for j in (0, 1) if j or k]
+    pairs.sort(key=lambda pair: (pair[1] < 2, -pair[0]))
+
+    rows, own_width = queries.shape
+    own_rows = heads.shape[0]
+    wide = query.shape[1]
+    group = wide // HEAD_WIDTH
+    tile = min(256, rows)
+    scale = HEAD_WIDTH ** (-0.5) * 1.4426950408889634
+    hidden = up_all.shape[1]
+    up_rows = up.shape[0]
+    out_cols = down.shape[1]
+
+    def block(index, size):
+        return pl.ds(pl.multiple_of(index * size, size), size)
+
+    loads = [
+        pltpu.make_async_copy(src, dst, load_sem.at[i])
+        for i, (src, dst) in enumerate((
+            (values.at[:, block(row, HEAD_WIDTH)], value_all.at[me]),
+            (keys, key_raw),
+            (queries, query_raw),
+            (up.at[:, block(row, hidden)], up_all.at[block(me, up_rows)]),
+            (down.at[block(row, hidden)], down_all.at[me]),
+            (residual, rest),
+            (out_weight, weight),
+        ))
+    ]
+    for load in loads:
+        load.start()
+
+    def inside(index):
+        return (index >= 0) & (index < depth)
+
+    barrier = pltpu.get_barrier_semaphore()
+    for j, k in pairs:
+        pl.semaphore_signal(barrier, inc=1, device_id={"sp": place[j], "tp": peer[k]}, device_id_type=MESH)
+    for step in (-1, 1):
+
+        @pl.when(inside(layer + step))
+        def _():
+            pl.semaphore_signal(barrier, inc=1, device_id={"sp": me + 2 * step}, device_id_type=MESH)
+
+    ends = jnp.where(layer > 0, 1, 0) + jnp.where(layer < depth - 1, 1, 0)
+    pl.semaphore_wait(barrier, len(pairs) + ends)
+
+    def spot(kind, c):
+        if kind == UP:
+            return up_all.at[block(c, up_rows)]
+        return {VALUE: value_all, KEY: key_all, DOWN: down_all}[kind].at[c]
+
+    def line(kind, way, step, part, sender):
+        sign = 2 * way - 1
+        line_row = part if kind == DOWN else side[part]
+        there = spot(kind, (layer + sign * (step - 1 if sender else step)) * 2 + line_row)
+        return pltpu.make_async_remote_copy(
+            src_ref=there,
+            dst_ref=there,
+            send_sem=line_send.at[kind, way, step - 1, part],
+            recv_sem=line_recv.at[kind, way, step - 1, part],
+            device_id={"sp": me - 2 * sign},
+            device_id_type=MESH,
+        )
+
+    def sends(way, step):
+        sign = 2 * way - 1
+        return inside(layer + sign * (step - 1)) & inside(layer - sign)
+
+    def launch(kind, part):
+        for way in (0, 1):
+
+            @pl.when(sends(way, 1))
+            def _():
+                line(kind, way, 1, part, True).start()
+
+    def relay(kind, step, part):
+        for way in (0, 1):
+
+            @pl.when(inside(layer + (2 * way - 1) * step))
+            def _():
+                line(kind, way, step, part, False).wait_recv()
+
+            if step < depth - 1:
+
+                @pl.when(sends(way, step + 1))
+                def _():
+                    line(kind, way, step + 1, part, True).start()
+
+    QUERY = 4
+
+    def swap(kind, sender):
+        source = {
+            VALUE: lambda: values.at[:, block(side[1], HEAD_WIDTH)],
+            KEY: lambda: key_spare,
+            UP: lambda: up.at[:, block(side[1], hidden)],
+            DOWN: lambda: down.at[block(side[1], hidden)],
+            QUERY: lambda: query_spare,
+        }[kind]()
+        turn = 0 if sender else 1
+        there = query.at[block(side[turn], rows)] if kind == QUERY else spot(kind, place[turn])
+        return pltpu.make_async_remote_copy(
+            src_ref=source,
+            dst_ref=there,
+            send_sem=swap_send.at[kind],
+            recv_sem=swap_recv.at[kind],
+            device_id={"sp": mate},
+            device_id_type=MESH,
+        )
+
+    def rotate(src, first_col, gain, dst, first_row, count):
+        lane = lax.broadcasted_iota(jnp.int32, (GRID_W, HEAD_WIDTH), 1)
+        even = (lane // (HEAD_WIDTH // 4)) % 2 == 0
+
+        def body(r, carry):
+            grid_row = me * (rows // GRID_W) + r
+            cosine = col_cos[...] + row_cos[pl.ds(grid_row, 1), :]
+            sine = col_sin[...] + row_sin[pl.ds(grid_row, 1), :]
+            here = block(r, GRID_W)
+            there = pl.ds(pl.multiple_of(first_row + r * GRID_W, GRID_W), GRID_W)
+            for h in range(count):
+                cols = pl.ds(pl.multiple_of(first_col + h * HEAD_WIDTH, HEAD_WIDTH), HEAD_WIDTH)
+                v = src[here, cols].astype(jnp.float32)
+                v = v * lax.rsqrt(jnp.mean(v * v, axis=-1, keepdims=True) + epsilon) * gain[...]
+                turned = jnp.where(
+                    even,
+                    pltpu.roll(v, HEAD_WIDTH - HEAD_WIDTH // 4, 1),
+                    pltpu.roll(v, HEAD_WIDTH // 4, 1),
+                )
+                dst[there, pl.ds(h * HEAD_WIDTH, HEAD_WIDTH)] = (v * cosine + turned * sine).astype(dst.dtype)
+            return carry
+
+        lax.fori_loop(0, rows // GRID_W, body, 0)
+
+    def flash(c, first, base, length):
+        def body(index, carry):
+            here = pl.ds(pl.multiple_of(base + index * tile, tile), tile)
+            key = key_all[c]
+            value = value_all[c]
+            columns = [pl.ds(g * HEAD_WIDTH, HEAD_WIDTH) for g in range(group)]
+            scores = [
+                lax.dot_general(
+                    query[here, cols], key, (((1,), (1,)), ((), ())), preferred_element_type=jnp.float32
+                )
+                for cols in columns
+            ]
+            for s, cols in zip(scores, columns):
+                top = jnp.max(s, axis=1, keepdims=True) * scale
+                if first:
+                    newest = jnp.broadcast_to(top, (tile, HEAD_WIDTH))
+                else:
+                    old = best[here, cols]
+                    newest = jnp.maximum(old, top)
+                    factor = jnp.exp2(old - newest)
+                p = jnp.exp2(s * scale - newest[:, :1])
+                total = jnp.sum(p, axis=1, keepdims=True)
+                part = jnp.dot(p.astype(jnp.bfloat16), value, preferred_element_type=jnp.float32)
+                best[here, cols] = newest
+                if first:
+                    mass[here, cols] = jnp.broadcast_to(total, (tile, HEAD_WIDTH))
+                    acc[here, cols] = part
+                else:
+                    mass[here, cols] = mass[here, cols] * factor + total
+                    acc[here, cols] = acc[here, cols] * factor + part
+            return carry
+
+        lax.fori_loop(0, length // tile, body, 0)
+
+    def each_way(step, line_row, work):
+        def body(way, carry):
+            index = layer + (2 * way - 1) * step
+
+            @pl.when(inside(index))
+            def _():
+                work(index * 2 + line_row)
+
+            return carry
+
+        lax.fori_loop(0, 2, body, 0)
+
+    def attend(step, part):
+        each_way(step, side[part], lambda c: flash(c, False, 0, 2 * rows))
+
+    def relay_pair(step, part):
+        relay(VALUE, step, part)
+        relay(KEY, step, part)
+
+    swap(VALUE, True).start()
+    loads[0].wait()
+    launch(VALUE, 0)
+    loads[1].wait()
+    rotate(key_raw, row * HEAD_WIDTH, key_gain, key_all.at[me], 0, 1)
+    launch(KEY, 0)
+    rotate(key_raw, side[1] * HEAD_WIDTH, key_gain, key_spare, 0, 1)
+    swap(KEY, True).start()
+    swap(VALUE, False).wait_recv()
+    launch(VALUE, 1)
+    loads[2].wait()
+    rotate(query_raw, side[1] * wide, query_gain, query_spare, 0, group)
+    swap(QUERY, True).start()
+    swap(KEY, False).wait_recv()
+    launch(KEY, 1)
+    swap(UP, True).start()
+    loads[3].wait()
+    launch(UP, 0)
+    rotate(query_raw, row * wide, query_gain, query, row * rows, group)
+    flash(me, True, row * rows, rows)
+    relay_pair(1, 0)
+    flash(mate, False, row * rows, rows)
+    swap(QUERY, False).wait_recv()
+    flash(me, True, side[1] * rows, rows)
+    flash(mate, False, side[1] * rows, rows)
+    events = [(step, part) for step in range(1, depth) for part in (0, 1)]
+    swap_started = False
+    for i, (step, part) in enumerate(events):
+        later = events[i + 1] if i + 1 < len(events) else None
+        if i and step == depth - 1:
+            relay_pair(step, part)
+        if later is not None and later[0] < depth - 1:
+            relay_pair(*later)
+        if (later is None or later[0] == depth - 1) and not swap_started:
+            swap_started = True
+            swap(UP, False).wait_recv()
+            launch(UP, 1)
+            relay(UP, 1, 0)
+            swap(DOWN, True).start()
+        attend(step, part)
+
+    width = own_width
+
+    def token_rows(j, k):
+        return block(side[j] * tp + peer[k], own_rows)
+
+    def head_copy(j, k, sender):
+        at = (row, rank) if sender else (side[j], peer[k])
+        cols = pl.ds(pl.multiple_of(at[1] * width + at[0] * wide, wide), wide)
+        index = j * tp + k - 1
+        return pltpu.make_async_remote_copy(
+            src_ref=attn.at[token_rows(j, k)],
+            dst_ref=heads.at[:, cols],
+            send_sem=head_send.at[index],
+            recv_sem=head_recv.at[index],
+            device_id={"sp": place[j], "tp": peer[k]},
+            device_id_type=MESH,
+        )
+
+    for j, k in pairs:
+        here = token_rows(j, k)
+        attn[here, :] = (acc[here, :] / mass[here, :]).astype(attn.dtype)
+        head_copy(j, k, True).start()
+    here = token_rows(0, 0)
+    heads[:, pl.ds(pl.multiple_of(rank * width + row * wide, wide), wide)] = (acc[here, :] / mass[here, :]).astype(heads.dtype)
+    relay(UP, 1, 1)
+    for load in loads[4:]:
+        load.wait()
+    for j, k in pairs:
+        head_copy(j, k, False).wait_recv()
+
+    features = middle.shape[1]
+    lanes = min(256, features)
+
+    def project(c, total):
+        cols = block(c, lanes)
+        made = rest[:, cols].astype(jnp.float32) + jnp.dot(
+            heads[...], weight[:, cols], preferred_element_type=jnp.float32
+        )
+        middle[:, cols] = made
+        return total + jnp.sum(made * made, axis=1, keepdims=True)
+
+    squares = lax.fori_loop(0, features // lanes, project, jnp.zeros((own_rows, 1), jnp.float32))
+    inverse = lax.rsqrt(squares / features + epsilon)
+
+    def normalize(c, carry):
+        cols = block(c, lanes)
+        normed[pl.ds(0, own_rows), cols] = (middle[:, cols] * inverse * norm_gain[:, cols]).astype(normed.dtype)
+        return carry
+
+    lax.fori_loop(0, features // lanes, normalize, 0)
+
+    def rows_of(j, k):
+        return pl.ds((j * tp + k) * own_rows, own_rows)
+
+    def norm_copy(j, k):
+        if k % 2:
+            source, target = (j, k - 1), (0, 1)
+        elif j:
+            source, target = (0, k), (1, 0)
+        else:
+            source, target = (0, 0), (0, k)
+        index = j * tp + k - 1
+        return pltpu.make_async_remote_copy(
+            src_ref=normed.at[rows_of(*source)],
+            dst_ref=normed.at[rows_of(j, k)],
+            send_sem=norm_send.at[index],
+            recv_sem=norm_recv.at[index],
+            device_id={"sp": place[target[0]], "tp": peer[target[1]]},
+            device_id_type=MESH,
+        )
+
+    for k in range(2, tp, 2):
+        norm_copy(0, k).start()
+    norm_copy(1, 0).start()
+    norm_copy(0, 1).start()
+    for step in range(2, depth - 1):
+        for part in (0, 1):
+            relay(UP, step, part)
+    swap(DOWN, False).wait_recv()
+    launch(DOWN, 0)
+    launch(DOWN, 1)
+    for k in range(2, tp, 2):
+        norm_copy(0, k).wait_recv()
+        norm_copy(1, k).start()
+        norm_copy(0, k + 1).start()
+    norm_copy(1, 0).wait_recv()
+    norm_copy(1, 1).start()
+    for part in (0, 1):
+        relay(UP, depth - 1, part)
+    for k in range(1, tp, 2):
+        norm_copy(0, k).wait_recv()
+
+    all_rows = 2 * tp * own_rows
+    row_tile = min(512, tp * own_rows)
+    hid_tile = min(256, hidden)
+    act = weight.at[pl.ds(0, all_rows), pl.ds(0, hidden)]
+
+    def units(j):
+        tiles = tp * own_rows // row_tile
+
+        def body(i, carry):
+            here = pl.ds(pl.multiple_of(j * tp * own_rows + (i % tiles) * row_tile, row_tile), row_tile)
+            cols = block(i // tiles, hid_tile)
+            total = jnp.dot(normed[here, :], up_all[:, cols], preferred_element_type=jnp.float32)
+            total = jnp.maximum(total, 0.0)
+            act[here, cols] = (total * total).astype(act.dtype)
+            return carry
+
+        lax.fori_loop(0, tiles * (hidden // hid_tile), body, 0)
+
+    units(0)
+    relay(DOWN, 1, 0)
+    for k in range(2, tp, 2):
+        norm_copy(1, k).wait_recv()
+        norm_copy(1, k + 1).start()
+    for k in range(1, tp, 2):
+        norm_copy(1, k).wait_recv()
+    units(1)
+
+    far = [(j, k) for j, k in pairs if k % 2 == 0]
+
+    def half_rows(j, k):
+        return pl.ds((j * (tp // 2) + k // 2) * own_rows, own_rows)
+
+    def core_copy(c, j, k):
+        index = j * (tp // 2) + k // 2
+        return pltpu.make_async_remote_copy(
+            src_ref=give.at[c, rows_of(j, k)],
+            dst_ref=sibling.at[c, half_rows(j, k)],
+            send_sem=core_send.at[c, index],
+            recv_sem=core_recv.at[c, index],
+            device_id={"tp": peer[1]},
+            device_id_type=MESH,
+        )
+
+    def part_copy(c, j, k):
+        index = far.index((j, k))
+        return pltpu.make_async_remote_copy(
+            src_ref=give.at[c, rows_of(j, k)],
+            dst_ref=take.at[c, pl.ds(index * own_rows, own_rows)],
+            send_sem=part_send.at[c, index],
+            recv_sem=part_recv.at[c, index],
+            device_id={"sp": place[j], "tp": peer[k]},
+            device_id_type=MESH,
+        )
+
+    def contribute(c):
+        def body(t, carry):
+            here = block(t, row_tile)
+            give[c, here, :] = jnp.dot(
+                act[here, :], down_all[c], preferred_element_type=jnp.float32
+            ).astype(give.dtype)
+            return carry
+
+        lax.fori_loop(0, all_rows // row_tile, body, 0)
+        for j in (0, 1):
+            for k in range(1, tp, 2):
+                core_copy(c, j, k).start()
+
+        def both(j, k):
+            core_copy(c, j, k + 1).wait_recv()
+            mine = give[c, rows_of(j, k), :].astype(jnp.float32)
+            return mine + sibling[c, half_rows(j, k), :].astype(jnp.float32)
+
+        for j, k in far:
+            give[c, rows_of(j, k), :] = both(j, k).astype(give.dtype)
+            part_copy(c, j, k).start()
+        middle[:, block(c, out_cols)] += both(0, 0)
+
+    def finish(c):
+        cols = block(c, out_cols)
+        total = middle[:, cols]
+        for index, (j, k) in enumerate(far):
+            part_copy(c, j, k).wait_recv()
+            total = total + take[c, pl.ds(index * own_rows, own_rows), :].astype(jnp.float32)
+        out[:, cols] = total.astype(out.dtype)
+
+    relay(DOWN, 1, 1)
+    for part in (0, 1):
+        contribute(layer * 2 + part)
+    for i, (step, part) in enumerate(events):
+        if i == len(events) - 1:
+            for r in (0, 1):
+                finish(layer * 2 + r)
+            for old_step, old_part in events[:-3]:
+                each_way(old_step, old_part, finish)
+        if i > 1:
+            relay(DOWN, step, part)
+        each_way(step, part, contribute)
+    for step, part in events[-3:]:
+        each_way(step, part, finish)
+
+    for kind in range(4):
+        for step in range(1, depth):
+            for part in (0, 1):
+                for way in (0, 1):
+
+                    @pl.when(sends(way, step))
+                    def _():
+                        line(kind, way, step, part, True).wait_send()
+
+    for kind in range(5):
+        swap(kind, True).wait_send()
+    for j, k in pairs:
+        head_copy(j, k, True).wait_send()
+        norm_copy(j, k).wait_send()
+
+    def drain(c, carry):
+        for j in (0, 1):
+            for k in range(1, tp, 2):
+                core_copy(c, j, k).wait_send()
+        for j, k in far:
+            part_copy(c, j, k).wait_send()
+        return carry
+
+    lax.fori_loop(0, 2 * depth, drain, 0)
+
+
+def paired_local(
+    depth, tp, residual_in, queries, keys, values, query_gain, key_norm_gain, out_weight, norm_gain, up_weight, down_weight
+):
+    count = 2 * depth
+    rows, width = queries.shape
+    own_rows, features = residual_in.shape
+    tables = rotary_tables(rows * count)
+    anywhere = pl.BlockSpec(memory_space=pl.ANY)
+    vmem = pl.BlockSpec(memory_space=pltpu.VMEM)
+    bf16, f32 = jnp.bfloat16, jnp.float32
+    dma = pltpu.SemaphoreType.DMA
+    wide = width // 2
+    hidden = up_weight.shape[1] // 2
+    out_cols = down_weight.shape[1]
+    group_rows = 2 * tp * own_rows
+    far = tp - 1
+    return pl.pallas_call(
+        functools.partial(paired_kernel, depth, tp),
+        out_shape=jax.ShapeDtypeStruct(residual_in.shape, bf16),
+        in_specs=[anywhere] * 4 + [vmem] * 6 + [anywhere, vmem, anywhere, anywhere],
+        out_specs=vmem,
+        scratch_shapes=[
+            pltpu.VMEM(keys.shape, bf16),
+            pltpu.VMEM((rows, HEAD_WIDTH), bf16),
+            pltpu.VMEM((count, rows, HEAD_WIDTH), bf16),
+            pltpu.VMEM((count, rows, HEAD_WIDTH), bf16),
+            pltpu.VMEM(queries.shape, bf16),
+            pltpu.VMEM((rows, wide), bf16),
+            pltpu.VMEM((2 * rows, wide), bf16),
+            pltpu.VMEM((2 * rows, wide), bf16),
+            pltpu.VMEM((2 * rows, wide), f32),
+            pltpu.VMEM((2 * rows, wide), f32),
+            pltpu.VMEM((2 * rows, wide), f32),
+            pltpu.VMEM((own_rows, width * tp), bf16),
+            pltpu.VMEM(out_weight.shape, bf16),
+            pltpu.VMEM(residual_in.shape, f32),
+            pltpu.VMEM((group_rows, features), bf16),
+            pltpu.VMEM((features, hidden), bf16),
+            pltpu.VMEM((count, hidden, out_cols), bf16),
+            pltpu.VMEM((count, group_rows, out_cols), bf16),
+            pltpu.VMEM((count, group_rows // 2, out_cols), bf16),
+            pltpu.VMEM((count, far * own_rows, out_cols), bf16),
+            pltpu.VMEM(residual_in.shape, bf16),
+            dma((7,)),
+            dma((4, 2, depth - 1, 2)),
+            dma((4, 2, depth - 1, 2)),
+            dma((5,)),
+            dma((5,)),
+            dma((2 * tp - 1,)),
+            dma((2 * tp - 1,)),
+            dma((2 * tp - 1,)),
+            dma((2 * tp - 1,)),
+            dma((count, tp)),
+            dma((count, tp)),
+            dma((count, far)),
+            dma((count, far)),
+        ],
+        compiler_params=pltpu.CompilerParams(
+            collective_id=0, has_side_effects=True, vmem_limit_bytes=67043328
+        ),
+        name="layer",
+    )(
+        residual_in, queries, keys, values, query_gain[None], key_norm_gain[None], *tables,
+        out_weight, norm_gain[None], up_weight, down_weight,
+    )
+
+
 def solution(mesh):
+    order = ring_order(mesh)
+    count, tp = mesh.shape["sp"], mesh.shape["tp"]
+
+    def step(*arrays):
+        kv_heads = arrays[2].shape[1] // HEAD_WIDTH
+        if plane_width(mesh) == 2 and count >= 6 and tp % 2 == 0 and kv_heads == 2:
+            return paired_local(count // 2, tp, *arrays)
+        return local(order, tp, *arrays)
+
     return jax.shard_map(
-        functools.partial(local, ring_order(mesh), mesh.shape["tp"]),
+        step,
         mesh=mesh,
         in_specs=(
             P(("sp", "tp"), None),

time: 257 us -> 232 us (0.903)
  Pallas kernels: 254 us -> 229 us
    pallas_call x1, Pallas kernels: 254 us -> 229 us  [paired_local(): pl.pallas_call(functools.partial(paired_kernel, depth, tp), out_shape=jax...]
where the time goes in v1:
time: 232 us
  Pallas kernels  229 us (99%)
    pallas_call x1, Pallas kernels, paired_local(): pl.pallas_call(functools.partial(paired_kernel, depth, tp), out_shape=jax...  229 us

profile of v1, /device:TPU:0, one launch (start us, length us, event | category | flops | bytes accessed | tf_op | source)
XLA Modules:
  0.0 231.7 jit_solution(2174751594438961125)
XLA Ops:
  0.0 229.4 %layer.1 = bf16[256,2048]{1,0:T(8,128)(2,1)} custom-call(bf16[256,2048]{1,0:T(8,128)(2,1)} %residual.1, bf16[1024,512]{1,0:T(8,128)(2,1)} %queries.1, bf16[1024,256]{1,0:T(8,128)(2,1)} %keys.1, bf16[1024,256]{1,0:T(8,128)(2,1)} %values.1, f32[1,128]{1,0:T(1,128)} %bitcast.4, f32[1,128]{1,0:T(1,128)} %bitcast.5, f32[128,128]{1,0:T(8,128)} %constant.8.clone.row_cos, ...), custom_call_target="tpu_custom_call" | custom-call | tf_op jit(solution)/shard_map/layer/pallas_call | solution.py:944
  229.4 2.3 copy.16

commit v2 on v1

--- a/solution.py
+++ b/solution.py
@@ -492,6 +492,7 @@
     hidden = up_all.shape[1]
     up_rows = up.shape[0]
     out_cols = down.shape[1]
+    half_cols = out_cols // 2
 
     def block(index, size):
         return pl.ds(pl.multiple_of(index * size, size), size)
@@ -531,10 +532,16 @@
             return up_all.at[block(c, up_rows)]
         return {VALUE: value_all, KEY: key_all, DOWN: down_all}[kind].at[c]
 
+    def pieces(kind, step, part):
+        return (1, 2) if kind == DOWN and step == depth - 1 and part else (part,)
+
     def line(kind, way, step, part, sender):
         sign = 2 * way - 1
-        line_row = part if kind == DOWN else side[part]
+        split = kind == DOWN and step == depth - 1 and part
+        line_row = min(part, 1) if kind == DOWN else side[part]
         there = spot(kind, (layer + sign * (step - 1 if sender else step)) * 2 + line_row)
+        if split:
+            there = there.at[:, pl.ds((part - 1) * half_cols, half_cols)]
         return pltpu.make_async_remote_copy(
             src_ref=there,
             dst_ref=there,
@@ -566,7 +573,8 @@
 
                 @pl.when(sends(way, step + 1))
                 def _():
-                    line(kind, way, step + 1, part, True).start()
+                    for piece in pieces(kind, step + 1, part):
+                        line(kind, way, step + 1, piece, True).start()
 
     QUERY = 4
 
@@ -614,18 +622,21 @@
         lax.fori_loop(0, rows // GRID_W, body, 0)
 
     def flash(c, first, base, length):
+        columns = [pl.ds(g * HEAD_WIDTH, HEAD_WIDTH) for g in range(group)]
+
         def body(index, carry):
-            here = pl.ds(pl.multiple_of(base + index * tile, tile), tile)
             key = key_all[c]
             value = value_all[c]
-            columns = [pl.ds(g * HEAD_WIDTH, HEAD_WIDTH) for g in range(group)]
-            scores = [
-                lax.dot_general(
-                    query[here, cols], key, (((1,), (1,)), ((), ())), preferred_element_type=jnp.float32
-                )
-                for cols in columns
-            ]
-            for s, cols in zip(scores, columns):
+            value = jnp.concatenate([value, jnp.ones_like(value)], axis=1)
+            chains = []
+            for u in range(2):
+                here = pl.ds(pl.multiple_of(base + (index * 2 + u) * tile, tile), tile)
+                for cols in columns:
+                    s = lax.dot_general(
+                        query[here, cols], key, (((1,), (1,)), ((), ())), preferred_element_type=jnp.float32
+                    )
+                    chains.append((here, cols, s))
+            for here, cols, s in chains:
                 top = jnp.max(s, axis=1, keepdims=True) * scale
                 if first:
                     newest = jnp.broadcast_to(top, (tile, HEAD_WIDTH))
@@ -634,18 +645,18 @@
                     newest = jnp.maximum(old, top)
                     factor = jnp.exp2(old - newest)
                 p = jnp.exp2(s * scale - newest[:, :1])
-                total = jnp.sum(p, axis=1, keepdims=True)
-                part = jnp.dot(p.astype(jnp.bfloat16), value, preferred_element_type=jnp.float32)
+                made = jnp.dot(p.astype(jnp.bfloat16), value, preferred_element_type=jnp.float32)
+                part, total = made[:, :HEAD_WIDTH], made[:, HEAD_WIDTH:]
                 best[here, cols] = newest
                 if first:
-                    mass[here, cols] = jnp.broadcast_to(total, (tile, HEAD_WIDTH))
+                    mass[here, cols] = total
                     acc[here, cols] = part
                 else:
                     mass[here, cols] = mass[here, cols] * factor + total
                     acc[here, cols] = acc[here, cols] * factor + part
             return carry
 
-        lax.fori_loop(0, length // tile, body, 0)
+        lax.fori_loop(0, length // (tile * 2), body, 0)
 
     def each_way(step, line_row, work):
         def body(way, carry):
@@ -761,27 +772,34 @@
     def rows_of(j, k):
         return pl.ds((j * tp + k) * own_rows, own_rows)
 
-    def norm_copy(j, k):
+    half_own = own_rows // 2
+
+    def norm_copy(j, k, h):
+        size = own_rows if k % 2 else half_own
         if k % 2:
             source, target = (j, k - 1), (0, 1)
-        elif j:
-            source, target = (0, k), (1, 0)
+        elif j and k:
+            source, target = ((1, 0), (0, k)) if h else ((0, k), (1, 0))
         else:
-            source, target = (0, 0), (0, k)
+            source, target = (0, 0), (j, k)
         index = j * tp + k - 1
         return pltpu.make_async_remote_copy(
-            src_ref=normed.at[rows_of(*source)],
-            dst_ref=normed.at[rows_of(j, k)],
-            send_sem=norm_send.at[index],
-            recv_sem=norm_recv.at[index],
+            src_ref=normed.at[pl.ds((source[0] * tp + source[1]) * own_rows + h * half_own, size)],
+            dst_ref=normed.at[pl.ds((j * tp + k) * own_rows + h * half_own, size)],
+            send_sem=norm_send.at[index, h],
+            recv_sem=norm_recv.at[index, h],
             device_id={"sp": place[target[0]], "tp": peer[target[1]]},
             device_id_type=MESH,
         )
 
-    for k in range(2, tp, 2):
-        norm_copy(0, k).start()
-    norm_copy(1, 0).start()
-    norm_copy(0, 1).start()
+    def norm_halves(k):
+        return (0,) if k % 2 else (0, 1)
+
+    for h in (0, 1):
+        for k in range(2, tp, 2):
+            norm_copy(0, k, h).start()
+        norm_copy(1, 0, 1 - h).start()
+    norm_copy(0, 1, 0).start()
     for step in range(2, depth - 1):
         for part in (0, 1):
             relay(UP, step, part)
@@ -789,15 +807,20 @@
     launch(DOWN, 0)
     launch(DOWN, 1)
     for k in range(2, tp, 2):
-        norm_copy(0, k).wait_recv()
-        norm_copy(1, k).start()
-        norm_copy(0, k + 1).start()
-    norm_copy(1, 0).wait_recv()
-    norm_copy(1, 1).start()
+        norm_copy(0, k, 0).wait_recv()
+        norm_copy(1, k, 0).start()
+    norm_copy(1, 0, 1).wait_recv()
+    for k in range(2, tp, 2):
+        norm_copy(1, k, 1).start()
+    for k in range(2, tp, 2):
+        norm_copy(0, k, 1).wait_recv()
+        norm_copy(0, k + 1, 0).start()
+    norm_copy(1, 0, 0).wait_recv()
+    norm_copy(1, 1, 0).start()
     for part in (0, 1):
         relay(UP, depth - 1, part)
     for k in range(1, tp, 2):
-        norm_copy(0, k).wait_recv()
+        norm_copy(0, k, 0).wait_recv()
 
     all_rows = 2 * tp * own_rows
     row_tile = min(512, tp * own_rows)
@@ -818,111 +841,133 @@
         lax.fori_loop(0, tiles * (hidden // hid_tile), body, 0)
 
     units(0)
-    relay(DOWN, 1, 0)
     for k in range(2, tp, 2):
-        norm_copy(1, k).wait_recv()
-        norm_copy(1, k + 1).start()
+        for h in (0, 1):
+            norm_copy(1, k, h).wait_recv()
+        norm_copy(1, k + 1, 0).start()
     for k in range(1, tp, 2):
-        norm_copy(1, k).wait_recv()
+        norm_copy(1, k, 0).wait_recv()
     units(1)
 
     far = [(j, k) for j, k in pairs if k % 2 == 0]
 
-    def half_rows(j, k):
-        return pl.ds((j * (tp // 2) + k // 2) * own_rows, own_rows)
-
-    def core_copy(c, j, k):
-        index = j * (tp // 2) + k // 2
+    pair_rows = 2 * own_rows
+
+    def columns_of(h):
+        return pl.ds(h * half_cols, half_cols)
+
+    def core_copy(c, t, h):
         return pltpu.make_async_remote_copy(
-            src_ref=give.at[c, rows_of(j, k)],
-            dst_ref=sibling.at[c, half_rows(j, k)],
-            send_sem=core_send.at[c, index],
-            recv_sem=core_recv.at[c, index],
+            src_ref=give.at[c, pl.ds(pl.multiple_of(t * pair_rows + own_rows, own_rows), own_rows), columns_of(h)],
+            dst_ref=sibling.at[c, block(t, own_rows), columns_of(h)],
+            send_sem=core_send.at[c, t, h],
+            recv_sem=core_recv.at[c, t, h],
             device_id={"tp": peer[1]},
             device_id_type=MESH,
         )
 
-    def part_copy(c, j, k):
+    def part_copy(c, j, k, h):
         index = far.index((j, k))
         return pltpu.make_async_remote_copy(
-            src_ref=give.at[c, rows_of(j, k)],
-            dst_ref=take.at[c, pl.ds(index * own_rows, own_rows)],
-            send_sem=part_send.at[c, index],
-            recv_sem=part_recv.at[c, index],
+            src_ref=give.at[c, rows_of(j, k), columns_of(h)],
+            dst_ref=take.at[c, pl.ds(index * own_rows, own_rows), columns_of(h)],
+            send_sem=part_send.at[c, index, h],
+            recv_sem=part_recv.at[c, index, h],
             device_id={"sp": place[j], "tp": peer[k]},
             device_id_type=MESH,
         )
 
-    def contribute(c):
-        def body(t, carry):
-            here = block(t, row_tile)
-            give[c, here, :] = jnp.dot(
-                act[here, :], down_all[c], preferred_element_type=jnp.float32
+    def contribute(c, halves=(0, 1)):
+        span = pl.ds(halves[0] * half_cols, len(halves) * half_cols)
+
+        def body(i, carry):
+            t = tp - 1 - i
+            here = block(t, pair_rows)
+            give[c, here, span] = jnp.dot(
+                act[here, :], down_all[c, :, span], preferred_element_type=jnp.float32
             ).astype(give.dtype)
+            for h in halves:
+                core_copy(c, t, h).start()
             return carry
 
-        lax.fori_loop(0, all_rows // row_tile, body, 0)
-        for j in (0, 1):
-            for k in range(1, tp, 2):
-                core_copy(c, j, k).start()
-
-        def both(j, k):
-            core_copy(c, j, k + 1).wait_recv()
-            mine = give[c, rows_of(j, k), :].astype(jnp.float32)
-            return mine + sibling[c, half_rows(j, k), :].astype(jnp.float32)
+        lax.fori_loop(0, tp, body, 0)
+
+        def both(j, k, h):
+            t = j * (tp // 2) + k // 2
+            core_copy(c, t, h).wait_recv()
+            mine = give[c, rows_of(j, k), columns_of(h)].astype(jnp.float32)
+            return mine + sibling[c, pl.ds(t * own_rows, own_rows), columns_of(h)].astype(jnp.float32)
 
         for j, k in far:
-            give[c, rows_of(j, k), :] = both(j, k).astype(give.dtype)
-            part_copy(c, j, k).start()
-        middle[:, block(c, out_cols)] += both(0, 0)
-
-    def finish(c):
-        cols = block(c, out_cols)
-        total = middle[:, cols]
-        for index, (j, k) in enumerate(far):
-            part_copy(c, j, k).wait_recv()
-            total = total + take[c, pl.ds(index * own_rows, own_rows), :].astype(jnp.float32)
-        out[:, cols] = total.astype(out.dtype)
-
-    relay(DOWN, 1, 1)
+            for h in halves:
+                give[c, rows_of(j, k), columns_of(h)] = both(j, k, h).astype(give.dtype)
+                part_copy(c, j, k, h).start()
+        for h in halves:
+            cols = pl.ds(pl.multiple_of(c * out_cols + h * half_cols, half_cols), half_cols)
+            middle[:, cols] += both(0, 0, h)
+
+    def finish(c, halves=(0, 1)):
+        for h in halves:
+            cols = pl.ds(pl.multiple_of(c * out_cols + h * half_cols, half_cols), half_cols)
+            total = middle[:, cols]
+            for index, (j, k) in enumerate(far):
+                part_copy(c, j, k, h).wait_recv()
+                total = total + take[c, pl.ds(index * own_rows, own_rows), columns_of(h)].astype(jnp.float32)
+            out[:, cols] = total.astype(out.dtype)
+
+    def line_done(kind, steps):
+        for step in steps:
+            for part in (0,) + pieces(kind, step, 1):
+                for way in (0, 1):
+
+                    @pl.when(sends(way, step))
+                    def _():
+                        line(kind, way, step, part, True).wait_send()
+
+    def drain(c):
+        for h in (0, 1):
+            for t in range(tp):
+                core_copy(c, t, h).wait_send()
+            for j, k in far:
+                part_copy(c, j, k, h).wait_send()
+
+    def settle(c):
+        finish(c)
+        drain(c)
+
+    steps = range(1, depth)
+    relay(DOWN, 1, 0)
     for part in (0, 1):
         contribute(layer * 2 + part)
     for i, (step, part) in enumerate(events):
-        if i == len(events) - 1:
-            for r in (0, 1):
-                finish(layer * 2 + r)
-            for old_step, old_part in events[:-3]:
-                each_way(old_step, old_part, finish)
-        if i > 1:
+        if step == depth - 1:
+            if not part:
+                for kind in (VALUE, KEY, UP):
+                    line_done(kind, steps)
+                for kind in range(5):
+                    swap(kind, True).wait_send()
+                for j, k in pairs:
+                    head_copy(j, k, True).wait_send()
+                    for h in norm_halves(k):
+                        norm_copy(j, k, h).wait_send()
+            else:
+                for r in (0, 1):
+                    settle(layer * 2 + r)
+                for event in events[:-4]:
+                    each_way(*event, settle)
+        if i:
             relay(DOWN, step, part)
-        each_way(step, part, contribute)
-    for step, part in events[-3:]:
-        each_way(step, part, finish)
-
-    for kind in range(4):
-        for step in range(1, depth):
-            for part in (0, 1):
-                for way in (0, 1):
-
-                    @pl.when(sends(way, step))
-                    def _():
-                        line(kind, way, step, part, True).wait_send()
-
-    for kind in range(5):
-        swap(kind, True).wait_send()
-    for j, k in pairs:
-        head_copy(j, k, True).wait_send()
-        norm_copy(j, k).wait_send()
-
-    def drain(c, carry):
-        for j in (0, 1):
-            for k in range(1, tp, 2):
-                core_copy(c, j, k).wait_send()
-        for j, k in far:
-            part_copy(c, j, k).wait_send()
-        return carry
-
-    lax.fori_loop(0, 2 * depth, drain, 0)
+        if step == depth - 1 and part:
+            each_way(step, part, functools.partial(contribute, halves=(0,)))
+            line_done(DOWN, steps[:-1])
+            each_way(*events[-4], settle)
+            relay(DOWN, step, 2)
+            each_way(step, part, functools.partial(contribute, halves=(1,)))
+        else:
+            each_way(step, part, contribute)
+    for event in events[-3:]:
+        each_way(*event, settle)
+    line_done(DOWN, steps[-1:])
 
 
 def paired_local(
@@ -941,7 +986,7 @@
     out_cols = down_weight.shape[1]
     group_rows = 2 * tp * own_rows
     far = tp - 1
-    return pl.pallas_call(
+    made = pl.pallas_call(
         functools.partial(paired_kernel, depth, tp),
         out_shape=jax.ShapeDtypeStruct(residual_in.shape, bf16),
         in_specs=[anywhere] * 4 + [vmem] * 6 + [anywhere, vmem, anywhere, anywhere],
@@ -969,18 +1014,18 @@
             pltpu.VMEM((count, far * own_rows, out_cols), bf16),
             pltpu.VMEM(residual_in.shape, bf16),
             dma((7,)),
-            dma((4, 2, depth - 1, 2)),
-            dma((4, 2, depth - 1, 2)),
+            dma((4, 2, depth - 1, 3)),
+            dma((4, 2, depth - 1, 3)),
             dma((5,)),
             dma((5,)),
             dma((2 * tp - 1,)),
             dma((2 * tp - 1,)),
-            dma((2 * tp - 1,)),
-            dma((2 * tp - 1,)),
-            dma((count, tp)),
-            dma((count, tp)),
-            dma((count, far)),
-            dma((count, far)),
+            dma((2 * tp - 1, 2)),
+            dma((2 * tp - 1, 2)),
+            dma((count, tp, 2)),
+            dma((count, tp, 2)),
+            dma((count, far, 2)),
+            dma((count, far, 2)),
         ],
         compiler_params=pltpu.CompilerParams(
             collective_id=0, has_side_effects=True, vmem_limit_bytes=67043328
@@ -990,6 +1035,20 @@
         residual_in, queries, keys, values, query_gain[None], key_norm_gain[None], *tables,
         out_weight, norm_gain[None], up_weight, down_weight,
     )
+    return pl.pallas_call(
+        hand_over,
+        out_shape=jax.ShapeDtypeStruct(made.shape, bf16),
+        in_specs=[vmem],
+        out_specs=anywhere,
+        scratch_shapes=[dma],
+        name="hand_over",
+    )(made)
+
+
+def hand_over(made, out, sem):
+    copy = pltpu.make_async_copy(made, out, sem)
+    copy.start()
+    copy.wait()
 
 
 def solution(mesh):

time: 232 us -> 223 us (0.961)
  Pallas kernels: 229 us -> 223 us
    pallas_call x1, Pallas kernels: 229 us -> 221 us  [paired_local(): pl.pallas_call(functools.partial(paired_kernel, depth, tp), out_shape=jax...]
where the time goes in v2:
time: 223 us
  Pallas kernels  223 us (100%)
    pallas_call x1, Pallas kernels, paired_local(): pl.pallas_call(functools.partial(paired_kernel, depth, tp), out_shape=jax...  221 us

profile of v2, /device:TPU:0, one launch (start us, length us, event | category | flops | bytes accessed | tf_op | source)
XLA Modules:
  0.0 223.2 jit_solution(7389441876881595490)
XLA Ops:
  0.0 220.9 %layer.1.made = bf16[256,2048]{1,0:T(8,128)(2,1)} custom-call(bf16[256,2048]{1,0:T(8,128)(2,1)} %residual.1, bf16[1024,512]{1,0:T(8,128)(2,1)} %queries.1, bf16[1024,256]{1,0:T(8,128)(2,1)} %keys.1, bf16[1024,256]{1,0:T(8,128)(2,1)} %values.1, f32[1,128]{1,0:T(1,128)} %bitcast.4, f32[1,128]{1,0:T(1,128)} %bitcast.5, f32[128,128]{1,0:T(8,128)} %constant.8.clone.row_cos, ...), custom_call_target="tpu_custom_call" | custom-call | tf_op jit(solution)/shard_map/layer/pallas_call | solution.py:989
  220.9 2.2 hand_over.1

commit v3 on v2

--- a/solution.py
+++ b/solution.py
@@ -470,7 +470,7 @@
     key_raw, key_spare, key_all, value_all, query_raw, query_spare, query, attn, acc, best, mass, heads,
     weight, middle, normed, up_all, down_all, give, sibling, take, rest,
     load_sem, line_send, line_recv, swap_send, swap_recv, head_send, head_recv, norm_send, norm_recv,
-    core_send, core_recv, part_send, part_recv,
+    core_send, core_recv, part_send, part_recv, shown, out_sem,
 ):
     me = lax.axis_index("sp")
     rank = lax.axis_index("tp")
@@ -906,6 +906,10 @@
             cols = pl.ds(pl.multiple_of(c * out_cols + h * half_cols, half_cols), half_cols)
             middle[:, cols] += both(0, 0, h)
 
+    def out_copy(c):
+        cols = block(c, out_cols)
+        return pltpu.make_async_copy(shown.at[:, cols], out.at[:, cols], out_sem.at[c])
+
     def finish(c, halves=(0, 1)):
         for h in halves:
             cols = pl.ds(pl.multiple_of(c * out_cols + h * half_cols, half_cols), half_cols)
@@ -913,7 +917,8 @@
             for index, (j, k) in enumerate(far):
                 part_copy(c, j, k, h).wait_recv()
                 total = total + take[c, pl.ds(index * own_rows, own_rows), columns_of(h)].astype(jnp.float32)
-            out[:, cols] = total.astype(out.dtype)
+            shown[:, cols] = total.astype(shown.dtype)
+        out_copy(c).start()
 
     def line_done(kind, steps):
         for step in steps:
@@ -969,6 +974,12 @@
         each_way(*event, settle)
     line_done(DOWN, steps[-1:])
 
+    def written(c, carry):
+        out_copy(c).wait()
+        return carry
+
+    lax.fori_loop(0, 2 * depth, written, 0)
+
 
 def paired_local(
     depth, tp, residual_in, queries, keys, values, query_gain, key_norm_gain, out_weight, norm_gain, up_weight, down_weight
@@ -990,7 +1001,7 @@
         functools.partial(paired_kernel, depth, tp),
         out_shape=jax.ShapeDtypeStruct(residual_in.shape, bf16),
         in_specs=[anywhere] * 4 + [vmem] * 6 + [anywhere, vmem, anywhere, anywhere],
-        out_specs=vmem,
+        out_specs=anywhere,
         scratch_shapes=[
             pltpu.VMEM(keys.shape, bf16),
             pltpu.VMEM((rows, HEAD_WIDTH), bf16),
@@ -1026,6 +1037,8 @@
             dma((count, tp, 2)),
             dma((count, far, 2)),
             dma((count, far, 2)),
+            pltpu.VMEM(residual_in.shape, bf16),
+            dma((count,)),
         ],
         compiler_params=pltpu.CompilerParams(
             collective_id=0, has_side_effects=True, vmem_limit_bytes=67043328
@@ -1038,17 +1051,25 @@
     return pl.pallas_call(
         hand_over,
         out_shape=jax.ShapeDtypeStruct(made.shape, bf16),
-        in_specs=[vmem],
+        in_specs=[anywhere],
         out_specs=anywhere,
-        scratch_shapes=[dma],
+        scratch_shapes=[pltpu.VMEM(made.shape, bf16), dma((2, 4))],
         name="hand_over",
     )(made)
 
 
-def hand_over(made, out, sem):
-    copy = pltpu.make_async_copy(made, out, sem)
-    copy.start()
-    copy.wait()
+def hand_over(made, out, held, sem):
+    size = made.shape[0] // 4
+    spans = [pl.ds(i * size, size) for i in range(4)]
+    taken = [pltpu.make_async_copy(made.at[span], held.at[span], sem.at[0, i]) for i, span in enumerate(spans)]
+    given = [pltpu.make_async_copy(held.at[span], out.at[span], sem.at[1, i]) for i, span in enumerate(spans)]
+    for copy in taken:
+        copy.start()
+    for take, give in zip(taken, given):
+        take.wait()
+        give.start()
+    for copy in given:
+        copy.wait()
 
 
 def solution(mesh):

time: 223 us -> 223 us (level)
  no operation moved by 1% of the time
where the time goes in v3:
time: 223 us
  Pallas kernels  223 us (100%)
    pallas_call x1, Pallas kernels, paired_local(): pl.pallas_call(functools.partial(paired_kernel, depth, tp), out_shape=jax...  221 us

profile of v3, /device:TPU:0, one launch (start us, length us, event | category | flops | bytes accessed | tf_op | source)
XLA Modules:
  0.0 222.8 jit_solution(4430626327549788215)
XLA Ops:
  0.0 220.6 %layer.1.made = bf16[256,2048]{1,0:T(8,128)(2,1)} custom-call(bf16[256,2048]{1,0:T(8,128)(2,1)} %residual.1, bf16[1024,512]{1,0:T(8,128)(2,1)} %queries.1, bf16[1024,256]{1,0:T(8,128)(2,1)} %keys.1, bf16[1024,256]{1,0:T(8,128)(2,1)} %values.1, f32[1,128]{1,0:T(1,128)} %bitcast.4, f32[1,128]{1,0:T(1,128)} %bitcast.5, f32[128,128]{1,0:T(8,128)} %constant.8.clone.row_cos, ...), custom_call_target="tpu_custom_call" | custom-call | tf_op jit(solution)/shard_map/layer/pallas_call | solution.py:1000
  220.6 2.0 hand_over.1
